TPU v7x, 32 devices: a whole 2x2x4 slice. The times are simulated.
32 devices in a mesh: sp: 16 (over z, y, x), tp: 2 (over core).
Axes of the slice: x: 2, y: 2, z: 4, core: 2. Of those that a mesh axis runs over, the one named last changes fastest.
Arguments:
- residual: bfloat16 [3072, 2048], P(('sp', 'tp')), may hold values from -6 to 6
- queries_narrow: bfloat16 [3072, 512], P('sp', 'tp'), may hold values from -24 to 24
- keys_narrow: bfloat16 [3072, 512], P('sp', 'tp'), may hold values from -24 to 24
- values_narrow: bfloat16 [3072, 512], P('sp', 'tp'), may hold values from -6 to 6
- queries_broad: bfloat16 [3072, 512], P('sp', 'tp'), may hold values from -24 to 24
- keys_broad: bfloat16 [3072, 512], P('sp', 'tp'), may hold values from -24 to 24
- values_broad: bfloat16 [3072, 512], P('sp', 'tp'), may hold values from -6 to 6
- gates_narrow: float32 [3072, 16], P('sp', 'tp'), may hold values from -3072 to 0, as said below
- gates_broad: float32 [3072, 8], P('sp', 'tp'), may hold values from -3072 to 0, as said below
- project_narrow: bfloat16 [512, 2048], P('tp'), may hold values from -0.5 to 0.5
- project_broad: bfloat16 [512, 2048], P('tp'), may hold values from -0.5 to 0.5
- norm_gain: float32 [2048], replicated, may hold values from 0.1 to 1.9
- up_weight: bfloat16 [2048, 8192], P('sp', 'tp'), may hold values from -0.125 to 0.125
- down_weight: bfloat16 [8192, 2048], P('tp', 'sp'), may hold values from -0.0625 to 0.0625
Outputs:
- layer_out: bfloat16 [3072, 2048], P(('sp', 'tp'))
Inputs may be any that keep to these rules, and one draw needn't show every extreme that they name: `gates_narrow`: each head's cumulative log gate never rises from one position to the next. `gates_broad`: each head's cumulative log gate never rises from one position to the next.
All inputs are finite; a program needn't handle non-finite values.
Results may differ from a plain program's by a relative error of at most 0.018.
Values may be sent and summed in bfloat16 or wider, within the bound.
A program may use at most 128 MiB of HBM per device.

v0:
```python
import jax
import jax.numpy as jnp
from jax import lax
from jax.sharding import PartitionSpec as P

A_DIM = 32
B_DIM = 64


def group_update(state, queries, keys, values, query_gates, key_gates, allowed, head_size):
    peak, total, summed = state
    query_count = queries.shape[0]
    key_count = keys.shape[0]
    heads = queries.shape[1] // head_size
    scores = jnp.einsum(
        "qhd,khd->hqk",
        queries.reshape(query_count, heads, head_size),
        keys.reshape(key_count, heads, head_size),
        preferred_element_type=jnp.float32,
    ) * head_size ** (-0.5)
    scores = scores + query_gates.T[:, :, None] - key_gates.T[:, None, :]
    scores = jnp.where(allowed[None], scores, -1e30)
    new_peak = jnp.maximum(peak, jnp.max(scores, axis=-1))
    weights = jnp.exp(scores - new_peak[..., None]) * allowed[None].astype(jnp.float32)
    total = jnp.sum(weights, axis=-1)
    summed = jnp.einsum(
        "hqk,khd->hqd",
        weights.astype(jnp.bfloat16),
        values.reshape(key_count, heads, head_size),
        preferred_element_type=jnp.float32,
    )
    return (new_peak, total, summed)


def empty_state(query_count, heads, head_size):
    return (
        jnp.full((heads, query_count), -1e30, jnp.float32),
        jnp.zeros((heads, query_count), jnp.float32),
        jnp.zeros((heads, query_count, head_size), jnp.float32),
    )


def finish_group(state, head_size):
    peak, total, summed = state
    result = summed / total[..., None]
    return (
        result.transpose(1, 0, 2)
        .reshape(result.shape[1], result.shape[0] * head_size)
        .astype(jnp.bfloat16)
    )


def rms_scaled(mixed, norm_gain):
    mixed_wide = mixed.astype(jnp.float32)
    scale = lax.rsqrt(jnp.mean(mixed_wide * mixed_wide, axis=-1, keepdims=True) + 1e-06)
    return (mixed_wide * scale * norm_gain).astype(jnp.bfloat16)


def local(
    residual,
    queries_narrow,
    keys_narrow,
    values_narrow,
    queries_broad,
    keys_broad,
    values_broad,
    gates_narrow,
    gates_broad,
    project_narrow,
    project_broad,
    norm_gain,
    up_weight,
    down_weight,
):
    local_count = queries_narrow.shape[0]
    table_narrow, table_broad = (
        lax.all_gather(gates_narrow, "sp", axis=0, tiled=True),
        lax.all_gather(gates_broad, "sp", axis=0, tiled=True),
    )
    query_pos = lax.axis_index("sp") * local_count + jnp.arange(local_count, dtype=jnp.int32)
    initial = (
        empty_state(local_count, queries_narrow.shape[1] // A_DIM, A_DIM),
        empty_state(local_count, queries_broad.shape[1] // B_DIM, B_DIM),
    )
    piece_keys_narrow = lax.all_gather(keys_narrow, "sp", axis=0, tiled=True)
    piece_values_narrow = lax.all_gather(values_narrow, "sp", axis=0, tiled=True)
    piece_keys_broad = lax.all_gather(keys_broad, "sp", axis=0, tiled=True)
    piece_values_broad = lax.all_gather(values_broad, "sp", axis=0, tiled=True)
    piece_count = piece_keys_narrow.shape[0]
    key_pos = jnp.arange(piece_count, dtype=jnp.int32)
    allowed = key_pos[None, :] <= query_pos[:, None]
    state_narrow = group_update(
        initial[0],
        queries_narrow,
        piece_keys_narrow,
        piece_values_narrow,
        gates_narrow,
        table_narrow,
        allowed,
        A_DIM,
    )
    state_broad = group_update(
        initial[1],
        queries_broad,
        piece_keys_broad,
        piece_values_broad,
        gates_broad,
        table_broad,
        allowed,
        B_DIM,
    )
    attended_narrow = finish_group(state_narrow, A_DIM)
    attended_broad = finish_group(state_broad, B_DIM)
    projected = lax.psum_scatter(
        (
            jnp.dot(attended_narrow, project_narrow, preferred_element_type=jnp.float32)
            + jnp.dot(attended_broad, project_broad, preferred_element_type=jnp.float32)
        ).astype(jnp.bfloat16),
        "tp",
        scatter_dimension=0,
        tiled=True,
    ).astype(jnp.float32)
    mixed = (residual.astype(jnp.float32) + projected).astype(jnp.bfloat16)
    features = lax.all_gather(rms_scaled(mixed, norm_gain), "tp", axis=0, tiled=True)
    up_total = jnp.dot(
        features,
        lax.all_gather(up_weight, "sp", axis=0, tiled=True),
        preferred_element_type=jnp.float32,
    )
    hidden = jnp.square(jax.nn.relu(up_total)).astype(jnp.bfloat16)
    down_term = jnp.dot(
        hidden,
        lax.all_gather(down_weight, "sp", axis=1, tiled=True),
        preferred_element_type=jnp.float32,
    )
    summed_rows = lax.psum_scatter(
        down_term.astype(jnp.bfloat16), "tp", scatter_dimension=0, tiled=True
    ).astype(jnp.float32)
    return (mixed.astype(jnp.float32) + summed_rows).astype(jnp.bfloat16)


def solution(mesh):
    return jax.shard_map(
        local,
        mesh=mesh,
        in_specs=(
            P(("sp", "tp"), None),
            P("sp", "tp"),
            P("sp", "tp"),
            P("sp", "tp"),
            P("sp", "tp"),
            P("sp", "tp"),
            P("sp", "tp"),
            P("sp", "tp"),
            P("sp", "tp"),
            P("tp", None),
            P("tp", None),
            P(),
            P("sp", "tp"),
            P("tp", "sp"),
        ),
        out_specs=P(("sp", "tp"), None),
        check_vma=False,
    )
```

profile of v0, /device:TPU:0, one launch (start us, length us, event | category | flops | bytes accessed | tf_op | source)
XLA Modules:
  0.0 742.3 jit_solution(3498710460941625432)
XLA Ops:
  6.5 0.7 all-gather.9.cloned.1.call-update
  7.3 0.0 all-gather.13.cloned.1.call-start
  7.3 0.7 all-gather.13.cloned.1.call-update
  8.0 0.0 all-gather.11.cloned.1.call-start
  8.1 0.7 all-gather.11.cloned.1.call-update
  8.7 0.0 all-gather.15.cloned.1.call-start
  8.8 0.5 all-gather.15.cloned.1.call-update
  9.3 0.0 reduce-scatter.3.cloned.1.call-start
  9.4 1.3 iota_compare_fusion
  10.7 43.5 %all-gather = f32[16,192,8]{1,2,0:T(8,128)S(1)} all-gather(f32[1,192,8]{1,2,0:T(8,128)} %bitcast.59), channel_id=1, replica_groups=mesh['sp'=16,'tp'=2] {'sp'}, dimensions={0}, use_global_device_ids=true | all-gather | bytes 104448 | tf_op jit(solution)/shard_map/all_gather | solution.py:77
  54.3 0.7 reshape.92
  55.0 1.7 copy.29
  56.7 36.3 %all-gather.1 = f32[16,192,4]{1,2,0:T(4,128)S(1)} all-gather(f32[1,192,4]{1,2,0:T(4,128)} %bitcast.65), channel_id=1, replica_groups=mesh['sp'=16,'tp'=2] {'sp'}, dimensions={0}, use_global_device_ids=true | all-gather | bytes 52224 | tf_op jit(solution)/shard_map/all_gather | solution.py:78
  93.0 0.1 reshape.94
  93.1 1.6 copy.33
  94.7 2.6 copy.30
  97.3 7.4 fusion.2
  104.8 6.4 copy-done.4
  111.2 0.4 copy-done.14
  111.5 8.6 %fusion = f32[8,192]{1,0:T(8,128)} fusion(f32[8,192,3072]{2,1,0:T(8,128)S(1)} %get-tuple-element.8, f32[192,3072]{1,0:T(8,128)S(1)} %get-tuple-element.6, f32[8,192]{1,0:T(8,128)S(1)} %broadcast_maximum_fusion, f32[8,3072]{1,0:T(8,128)S(1)} %bitcast.53, f32[8,192]{1,0:T(8,128)S(1)} %bitcast.61, pred[192,3072]{1,0:T(8,128)(4,1)S(1)} %copy-done.8), kind=kLoop, calls=%fused_computation.2 | loop fusion | flops 33028608 | bytes 21940224 | tf_op jit(solution)/shard_map/reduce_sum | solution.py:25
  120.2 10.4 %all-gather.13.cloned.1.call-done = bf16[3072,256]{1,0:T(8,128)(2,1)} async-done(((bf16[192,256]{1,0:T(8,128)(2,1)}), bf16[3072,256]{1,0:T(8,128)(2,1)}) %all-gather.13.cloned.1.call-update) | async-done | bytes 1572880 | tf_op jit(solution)/shard_map/all_gather | solution.py:87
  130.6 2.6 copy.34
  133.2 8.0 %fusion.41 = (f32[4,192]{1,0:T(4,128)S(1)}, f32[4,192,3072]{2,1,0:T(8,128)}) fusion(f32[4,3072]{1,0:T(4,128)S(1)} %bitcast.58, f32[4,192]{1,0:T(4,128)} %bitcast.66, bf16[192,4,64]{0,2,1:T(8,128)(2,1)} %bitcast.55, bf16[3072,4,64]{0,2,1:T(8,128)(2,1)} %bitcast.49, pred[192,3072]{1,0:T(8,128)(4,1)} %get-tuple-element.5), kind=kOutput, calls=%fused_computation.43 | convolution fusion | flops 313785600 | bytes 11753472 | tf_op jit(solution)/shard_map/qhd,khd->hqk/dot_general | solution.py:15
  141.1 48.9 %all-gather.11.cloned.1.call-done = bf16[3072,256]{1,0:T(8,128)(2,1)} async-done(((bf16[192,256]{1,0:T(8,128)(2,1)}), bf16[3072,256]{1,0:T(8,128)(2,1)}) %all-gather.11.cloned.1.call-update) | async-done | bytes 1572880 | tf_op jit(solution)/shard_map/all_gather | solution.py:86
  190.1 2.7 copy.32
  192.8 11.0 %fusion.24 = bf16[192,8,32]{0,2,1:T(8,128)(2,1)S(1)} fusion(bf16[3072,8,32]{0,2,1:T(8,128)(2,1)} %bitcast.48, f32[8,192,3072]{2,1,0:T(8,128)} %copy-done.4, f32[192,3072]{1,0:T(8,128)} %copy-done.2, f32[8,192]{1,0:T(8,128)S(1)} %copy-done.15, f32[8,3072]{1,0:T(8,128)S(1)} %bitcast.54, f32[8,192]{1,0:T(8,128)S(1)} %bitcast.62, ...), kind=kOutput, calls=%fused_computation.27 | convolution fusion | flops 335118336 | bytes 23611392 | tf_op jit(solution)/shard_map/hqk,khd->hqd/dot_general | solution.py:26
  203.8 1.6 fusion.42
  205.4 1.8 fusion.6
  207.3 42.1 %all-gather.15.cloned.1.call-done = bf16[3072,256]{1,0:T(8,128)(2,1)} async-done(((bf16[192,256]{1,0:T(8,128)(2,1)}), bf16[3072,256]{1,0:T(8,128)(2,1)}) %all-gather.15.cloned.1.call-update) | async-done | bytes 1572880 | tf_op jit(solution)/shard_map/all_gather | solution.py:88
  249.4 2.6 copy.36
  252.0 6.7 fusion.30
  258.8 1.3 fusion.14
  260.1 0.0 reduce-scatter.3.cloned.1.call-update
  260.1 0.0 all-gather.17.cloned.1.call-start
  260.2 0.5 all-gather.17.cloned.1.call-update
  260.7 0.0 all-gather.19.cloned.1.call-start
  260.7 0.7 all-gather.19.cloned.1.call-update
  261.4 0.0 reduce-scatter.5.cloned.1.call-start
  261.5 5.7 reduce-scatter.3.cloned.1.call-done
  267.1 1.2 fusion.33
  268.4 1.2 fusion.35
  269.6 2.4 all_gather.33
  271.9 190.0 %all-gather.17.cloned.1.call-done = bf16[2048,4096]{1,0:T(8,128)(2,1)} async-done(((bf16[128,4096]{1,0:T(8,128)(2,1)}), bf16[2048,4096]{1,0:T(8,128)(2,1)}) %all-gather.17.cloned.1.call-update) | async-done | bytes 16777232 | tf_op jit(solution)/shard_map/all_gather | solution.py:127
  461.9 250.0 %all-gather.19.cloned.1.call-done = bf16[4096,2048]{1,0:T(8,128)(2,1)} async-done(((bf16[4096,128]{1,0:T(8,128)(2,1)}), bf16[4096,2048]{1,0:T(8,128)(2,1)}) %all-gather.19.cloned.1.call-update) | async-done | bytes 16777232 | tf_op jit(solution)/shard_map/all_gather | solution.py:133
  711.9 15.1 %convolution_convert_fusion = bf16[192,2048]{1,0:T(8,128)(2,1)} fusion(bf16[4096,2048]{1,0:T(8,128)(2,1)} %all-gather.19.cloned.1.call-done, bf16[192,2048]{1,0:T(8,128)(2,1)S(1)} %all_gather.33, bf16[2048,4096]{1,0:T(8,128)(2,1)} %all-gather.17.cloned.1.call-done), kind=kOutput, calls=%fused_computation.18 | convolution fusion | flops 6445203456 | bytes 35127296 | tf_op jit(solution)/shard_map/dot_general | solution.py:131
  727.0 0.0 reduce-scatter.5.cloned.1.call-update
  727.0 6.5 reduce-scatter.5.cloned.1.call-done
  733.5 1.9 fusion.36
  (49 shorter events, 0.2 us)
Async XLA Ops:
  6.5 197.3 %copy-start = (bf16[256,2048]{1,0:T(8,128)(2,1)S(1)}, bf16[256,2048]{1,0:T(8,128)(2,1)}, u32[]{:S(2)}) copy-start(bf16[256,2048]{1,0:T(8,128)(2,1)} %param.23) | copy-start | bytes 3145732
  6.5 88.2 %all-gather.9.cloned.1.call-start = ((), (), s32[]{:S(2)}) async-start(), calls=%async_computation.2 | async-start | bytes 1671168 | tf_op jit(solution)/shard_map/all_gather | solution.py:85
  7.3 123.3 %all-gather.13.cloned.1.call-start = ((), (), s32[]{:S(2)}) async-start(), calls=%async_computation.4 | async-start | bytes 1671168 | tf_op jit(solution)/shard_map/all_gather | solution.py:87
  8.0 182.0 %all-gather.11.cloned.1.call-start = ((), (), s32[]{:S(2)}) async-start(), calls=%async_computation.3 | async-start | bytes 1671168 | tf_op jit(solution)/shard_map/all_gather | solution.py:86
  8.7 240.7 %all-gather.15.cloned.1.call-start = ((), (), s32[]{:S(2)}) async-start(), calls=%async_computation.5 | async-start | bytes 1671168 | tf_op jit(solution)/shard_map/all_gather | solution.py:88
  9.3 257.8 %reduce-scatter.3.cloned.1.call-start = ((), (), s32[]{:S(2)}) async-start(), calls=%async_computation.6 | async-start | bytes 1179648 | tf_op jit(solution)/shard_map/reduce_scatter | solution.py:114
  10.7 94.0 %copy-start.2 = (f32[192,3072]{1,0:T(8,128)}, f32[192,3072]{1,0:T(8,128)S(1)}, u32[]{:S(2)}) copy-start(f32[192,3072]{1,0:T(8,128)S(1)} %get-tuple-element.6) | copy-start | bytes 7077892
  97.3 14.2 %copy-start.8 = (pred[192,3072]{1,0:T(8,128)(4,1)S(1)}, pred[192,3072]{1,0:T(8,128)(4,1)}, u32[]{:S(2)}) copy-start(pred[192,3072]{1,0:T(8,128)(4,1)} %get-tuple-element.5) | copy-start | bytes 1769476
  97.3 14.2 %copy-start.11 = (f32[3072,8]{0,1:T(8,128)S(1)}, f32[3072,8]{0,1:T(8,128)}, u32[]{:S(2)}) copy-start(f32[3072,8]{0,1:T(8,128)} %reshape.92) | copy-start | bytes 294916
  97.3 14.2 %copy-start.12 = (f32[192,8]{0,1:T(8,128)S(1)}, f32[192,8]{0,1:T(8,128)}, u32[]{:S(2)}) copy-start(f32[192,8]{0,1:T(8,128)} %param.21) | copy-start | bytes 18436
  104.7 6.4 copy-start.4
  104.7 6.8 copy-start.14
  133.2 59.6 %copy-start.9 = (pred[192,3072]{1,0:T(8,128)(4,1)S(1)}, pred[192,3072]{1,0:T(8,128)(4,1)}, u32[]{:S(2)}) copy-start(pred[192,3072]{1,0:T(8,128)(4,1)} %get-tuple-element.5) | copy-start | bytes 1769476
  133.2 59.6 %copy-start.13 = (f32[192,8]{0,1:T(8,128)S(1)}, f32[192,8]{0,1:T(8,128)}, u32[]{:S(2)}) copy-start(f32[192,8]{0,1:T(8,128)} %param.21) | copy-start | bytes 18436
  133.2 59.6 %copy-start.15 = (f32[8,192]{1,0:T(8,128)S(1)}, f32[8,192]{1,0:T(8,128)}, u32[]{:S(2)}) copy-start(f32[8,192]{1,0:T(8,128)} %copy-done.14) | copy-start | bytes 18436
  133.2 59.6 %copy-start.17 = (f32[8,192]{1,0:T(8,128)S(1)}, f32[8,192]{1,0:T(8,128)}, u32[]{:S(2)}) copy-start(f32[8,192]{1,0:T(8,128)} %fusion) | copy-start | bytes 18436
  190.0 15.4 %slice-start = ((s8[9437184]{0:T(1024)(128)(4,1)}), s8[1048576]{0:T(1024)(128)(4,1)S(1)}, s32[]{:S(2)}) async-start(s8[9437184]{0:T(1024)(128)(4,1)} %bitcast.45), calls=%async_computation.10 | async-start | bytes 2097152
  192.8 12.6 %slice-start.1 = ((s8[9437184]{0:T(1024)(128)(4,1)}), s8[4194304]{0:T(1024)(128)(4,1)S(1)}, s32[]{:S(2)}) async-start(s8[9437184]{0:T(1024)(128)(4,1)} %bitcast.45), calls=%async_computation.11 | async-start | bytes 8388608
  192.8 12.6 %slice-start.2 = ((s8[9437184]{0:T(1024)(128)(4,1)}), s8[4194304]{0:T(1024)(128)(4,1)S(1)}, s32[]{:S(2)}) async-start(s8[9437184]{0:T(1024)(128)(4,1)} %bitcast.45), calls=%async_computation.12 | async-start | bytes 8388608
  192.8 12.6 %copy-start.3 = (f32[192,3072]{1,0:T(8,128)S(1)}, f32[192,3072]{1,0:T(8,128)}, u32[]{:S(2)}) copy-start(f32[192,3072]{1,0:T(8,128)} %copy-done.2) | copy-start | bytes 7077892
  207.3 51.5 %copy-start.5 = (f32[192,2048]{1,0:T(8,128)S(1)}, f32[192,2048]{1,0:T(8,128)}, u32[]{:S(2)}) copy-start(f32[192,2048]{1,0:T(8,128)} %fusion.42) | copy-start | bytes 4718596
  207.3 51.5 %copy-start.10 = (bf16[256,2048]{1,0:T(8,128)(2,1)S(1)}, bf16[256,2048]{1,0:T(8,128)(2,1)}, u32[]{:S(2)}) copy-start(bf16[256,2048]{1,0:T(8,128)(2,1)} %param.24) | copy-start | bytes 3145732
  252.0 15.1 %copy-start.6 = (bf16[96,2048]{1,0:T(8,128)(2,1)S(1)}, bf16[96,2048]{1,0:T(8,128)(2,1)}, u32[]{:S(2)}) copy-start(bf16[96,2048]{1,0:T(8,128)(2,1)} %param.14) | copy-start | bytes 1179652
  252.0 16.4 %copy-start.16 = (f32[2048]{0:T(1024)S(1)}, f32[2048]{0:T(1024)}, u32[]{:S(2)}) copy-start(f32[2048]{0:T(1024)} %param.25) | copy-start | bytes 24580
  260.1 201.8 %all-gather.17.cloned.1.call-start = ((), (), s32[]{:S(2)}) async-start(), calls=%async_computation.7 | async-start | bytes 17825792 | tf_op jit(solution)/shard_map/all_gather | solution.py:127
  260.7 451.2 %all-gather.19.cloned.1.call-start = ((), (), s32[]{:S(2)}) async-start(), calls=%async_computation.8 | async-start | bytes 17825792 | tf_op jit(solution)/shard_map/all_gather | solution.py:133
  261.4 472.1 %reduce-scatter.5.cloned.1.call-start = ((), (), s32[]{:S(2)}) async-start(), calls=%async_computation.9 | async-start | bytes 1179648 | tf_op jit(solution)/shard_map/reduce_scatter | solution.py:136
  271.9 461.6 %copy-start.7 = (bf16[96,2048]{1,0:T(8,128)(2,1)S(1)}, bf16[96,2048]{1,0:T(8,128)(2,1)}, u32[]{:S(2)}) copy-start(bf16[96,2048]{1,0:T(8,128)(2,1)} %reduce-scatter.3.cloned.1.call-done) | copy-start | bytes 1179652
  711.9 23.5 %copy-start.1 = (bf16[256,2048]{1,0:T(8,128)(2,1)S(1)}, bf16[256,2048]{1,0:T(8,128)(2,1)}, u32[]{:S(2)}) copy-start(bf16[256,2048]{1,0:T(8,128)(2,1)} %param.23) | copy-start | bytes 3145732
Sparse Core Ops, SparseCore 0:
  10.1 60.9 all-gather.8
  73.8 56.6 all-gather.12
  133.3 56.6 all-gather.10
  192.7 56.7 all-gather.14
  260.2 6.8 reduce-scatter.2
  269.8 192.1 all-gather.16
  464.6 247.2 all-gather.18
  727.2 6.3 reduce-scatter.4
where the time goes:
time: 743 us; the launch traced here: 742 us
  waiting for transfers between devices  557 us (75%)
  blocking collectives  82.2 us (11%)
  matrix products  51.1 us (7%)
  local copies, waits for them, and re-layouts  21.5 us (3%)
  other arithmetic  16.1 us (2%)
  between operations  13.7 us (2%)
    all_gather x1, waiting for transfers between devices, local(): lax.all_gather(down_weight, 'sp', axis=1, tiled=True)  250 us
    all_gather x1, waiting for transfers between devices, local(): lax.all_gather(up_weight, 'sp', axis=0, tiled=True)  190 us
    all_gather x1, waiting for transfers between devices, local(): lax.all_gather(values_narrow, 'sp', axis=0, tiled=True)  48.9 us
    all_gather x1, blocking collectives, local(): lax.all_gather(gates_narrow, 'sp', axis=0, tiled=True)  43.5 us
    all_gather x1, waiting for transfers between devices, local(): piece_values_broad = lax.all_gather(values_broad, 'sp', axis=0, tiled=True)  42.1 us
    all_gather x1, blocking collectives, local(): lax.all_gather(gates_broad, 'sp', axis=0, tiled=True)  36.3 us
    dot_general x2, matrix products, group_update(): jnp.einsum('hqk,khd->hqd', weights.astype(jnp.bfloat16), values.reshape(k...  17.7 us
    dot_general x2, matrix products, group_update(): jnp.einsum('qhd,khd->hqk', queries.reshape(query_count, heads, head_size)...  15.4 us
  transfers between devices with their start and end apart: 8, of which 7 were waited for; matrix products, arithmetic and copies ran while one was open for 7% of the time, Pallas kernels for 0%

commit v1 on v0

--- a/solution.py
+++ b/solution.py
@@ -1,6 +1,10 @@
+import functools
+
 import jax
 import jax.numpy as jnp
 from jax import lax
+from jax.experimental import pallas as pl
+from jax.experimental.pallas import tpu as pltpu
 from jax.sharding import PartitionSpec as P
 
 A_DIM = 32
@@ -56,6 +60,270 @@
     return (mixed_wide * scale * norm_gain).astype(jnp.bfloat16)
 
 
+def group_size(sp_count):
+    return 8 if sp_count % 8 == 0 else sp_count
+
+
+def weights_kernel(
+    count, group, up_ref, down_ref, up_out, down_out, up_hold, down_hold, sems, own_sems
+):
+    me = lax.axis_index("sp")
+    up_rows = up_ref.shape[0]
+    units = up_out.shape[1]
+    columns = down_ref.shape[1]
+    barrier = pltpu.get_barrier_semaphore()
+
+    def hello(k, carry):
+        pl.semaphore_signal(
+            barrier,
+            inc=1,
+            device_id={"sp": (me + k) % count},
+            device_id_type=pl.DeviceIdType.MESH,
+        )
+        return carry
+
+    lax.fori_loop(1, count, hello, 0)
+    pl.semaphore_wait(barrier, count - 1)
+
+    def up_source(chunk):
+        return up_ref.at[:, pl.ds(pl.multiple_of(chunk * units, 128), units)]
+
+    def down_source(chunk):
+        return down_ref.at[pl.ds(pl.multiple_of(chunk * units, units), units), :]
+
+    def up_target(owner):
+        return up_out.at[pl.ds(pl.multiple_of(owner * up_rows, up_rows), up_rows), :]
+
+    def down_target(owner):
+        if len(down_out.shape) == 3:
+            return down_out.at[owner]
+        return down_out.at[:, pl.ds(pl.multiple_of(owner * columns, columns), columns)]
+
+    def copies(k, target_owner):
+        peer = (me + k) % count
+        chunk = peer % group
+        pairs = (
+            (up_source(chunk), up_target(target_owner)),
+            (down_source(chunk), down_target(target_owner)),
+        )
+        return [
+            pltpu.make_async_remote_copy(
+                src_ref=source,
+                dst_ref=target,
+                send_sem=sems.at[0, which, k],
+                recv_sem=sems.at[1, which, k],
+                device_id={"sp": peer},
+                device_id_type=pl.DeviceIdType.MESH,
+            )
+            for which, (source, target) in enumerate(pairs)
+        ]
+
+    def start(k, carry):
+        for copy in copies(k, me):
+            copy.start()
+        return carry
+
+    def finish(k, carry):
+        for copy in copies(k, (me + count - k) % count):
+            copy.wait_recv()
+            copy.wait_send()
+        return carry
+
+    lax.fori_loop(1, count, start, 0)
+    own = me % group
+    first = [
+        pltpu.make_async_copy(up_source(own), up_hold, own_sems.at[0]),
+        pltpu.make_async_copy(down_source(own), down_hold, own_sems.at[1]),
+    ]
+    for copy in first:
+        copy.start()
+    for copy in first:
+        copy.wait()
+    second = [
+        pltpu.make_async_copy(up_hold, up_target(me), own_sems.at[0]),
+        pltpu.make_async_copy(down_hold, down_target(me), own_sems.at[1]),
+    ]
+    for copy in second:
+        copy.start()
+    for copy in second:
+        copy.wait()
+    lax.fori_loop(1, count, finish, 0)
+
+
+def share_weights(up_weight, down_weight):
+    count = lax.axis_size("sp")
+    group = group_size(count)
+    up_rows, unit_total = up_weight.shape
+    columns = down_weight.shape[1]
+    units = unit_total // group
+    if columns % 128 == 0:
+        down_shape = (units, count * columns)
+    else:
+        down_shape = (count, units, columns)
+    up_full, down_full = pl.pallas_call(
+        functools.partial(weights_kernel, count, group),
+        out_shape=(
+            jax.ShapeDtypeStruct((count * up_rows, units), up_weight.dtype),
+            jax.ShapeDtypeStruct(down_shape, down_weight.dtype),
+        ),
+        in_specs=[pl.BlockSpec(memory_space=pl.ANY)] * 2,
+        out_specs=[pl.BlockSpec(memory_space=pl.ANY)] * 2,
+        scratch_shapes=[
+            pltpu.VMEM((up_rows, units), up_weight.dtype),
+            pltpu.VMEM((units, columns), down_weight.dtype),
+            pltpu.SemaphoreType.DMA((2, 2, count)),
+            pltpu.SemaphoreType.DMA((2,)),
+        ],
+        compiler_params=pltpu.CompilerParams(collective_id=0, has_side_effects=True),
+        cost_estimate=pl.CostEstimate(
+            flops=0, bytes_accessed=count * up_rows * units * 80, transcendentals=0
+        ),
+    )(up_weight, down_weight)
+    if columns % 128:
+        down_full = down_full.transpose(1, 0, 2).reshape(units, count * columns)
+    return up_full, down_full
+
+
+def gather_kernel(group, tp_count, rows_ref, out_ref, hold, sems, own_sems, pass_sems):
+    sp = lax.axis_index("sp")
+    tp = lax.axis_index("tp")
+    base = (sp // group) * group
+    me = sp - base
+    barrier = pltpu.get_barrier_semaphore()
+    for k in range(1, group):
+        pl.semaphore_signal(
+            barrier,
+            inc=1,
+            device_id={"sp": base + (me + k) % group},
+            device_id_type=pl.DeviceIdType.MESH,
+        )
+    for j in range(1, tp_count):
+        pl.semaphore_signal(
+            barrier,
+            inc=1,
+            device_id={"tp": (tp + j) % tp_count},
+            device_id_type=pl.DeviceIdType.MESH,
+        )
+    pl.semaphore_wait(barrier, group + tp_count - 2)
+
+    def across(k, owner):
+        return pltpu.make_async_remote_copy(
+            src_ref=rows_ref,
+            dst_ref=out_ref.at[tp, owner],
+            send_sem=sems.at[0, k],
+            recv_sem=sems.at[1, k],
+            device_id={"sp": base + (me + k) % group},
+            device_id_type=pl.DeviceIdType.MESH,
+        )
+
+    def beside(j, k, source, tp_owner, owner):
+        return pltpu.make_async_remote_copy(
+            src_ref=source,
+            dst_ref=out_ref.at[tp_owner, owner],
+            send_sem=pass_sems.at[0, j, k],
+            recv_sem=pass_sems.at[1, j, k],
+            device_id={"tp": (tp + j) % tp_count},
+            device_id_type=pl.DeviceIdType.MESH,
+        )
+
+    for k in range(1, group):
+        across(k, me).start()
+    for j in range(1, tp_count):
+        beside(j, 0, rows_ref, tp, me).start()
+    own = pltpu.make_async_copy(rows_ref, hold, own_sems.at[0])
+    own.start()
+    own.wait()
+    own = pltpu.make_async_copy(hold, out_ref.at[tp, me], own_sems.at[1])
+    own.start()
+    own.wait()
+    for k in range(1, group):
+        owner = (me + group - k) % group
+        across(k, owner).wait_recv()
+        for j in range(1, tp_count):
+            beside(j, k, out_ref.at[tp, owner], tp, owner).start()
+    for k in range(1, group):
+        across(k, me).wait_send()
+    for j in range(1, tp_count):
+        for k in range(group):
+            owner = (me + group - k) % group
+            copy = beside(j, k, rows_ref, (tp + tp_count - j) % tp_count, owner)
+            copy.wait_send()
+            copy.wait_recv()
+
+
+def gather_rows(rows):
+    group = group_size(lax.axis_size("sp"))
+    tp_count = lax.axis_size("tp")
+    return pl.pallas_call(
+        functools.partial(gather_kernel, group, tp_count),
+        out_shape=jax.ShapeDtypeStruct((tp_count, group) + rows.shape, rows.dtype),
+        in_specs=[pl.BlockSpec(memory_space=pl.ANY)],
+        out_specs=pl.BlockSpec(memory_space=pl.ANY),
+        scratch_shapes=[
+            pltpu.VMEM(rows.shape, rows.dtype),
+            pltpu.SemaphoreType.DMA((2, group)),
+            pltpu.SemaphoreType.DMA((2,)),
+            pltpu.SemaphoreType.DMA((2, tp_count, group)),
+        ],
+        compiler_params=pltpu.CompilerParams(collective_id=1, has_side_effects=True),
+    )(rows)
+
+
+def return_kernel(group, parts_ref, out_ref, hold, sems, own_sems):
+    sp = lax.axis_index("sp")
+    base = (sp // group) * group
+    me = sp - base
+    barrier = pltpu.get_barrier_semaphore()
+    for k in range(1, group):
+        pl.semaphore_signal(
+            barrier,
+            inc=1,
+            device_id={"sp": base + (me + k) % group},
+            device_id_type=pl.DeviceIdType.MESH,
+        )
+    pl.semaphore_wait(barrier, group - 1)
+
+    def across(k, owner):
+        peer = (me + k) % group
+        return pltpu.make_async_remote_copy(
+            src_ref=parts_ref.at[peer],
+            dst_ref=out_ref.at[owner],
+            send_sem=sems.at[0, k],
+            recv_sem=sems.at[1, k],
+            device_id={"sp": base + peer},
+            device_id_type=pl.DeviceIdType.MESH,
+        )
+
+    for k in range(1, group):
+        across(k, me).start()
+    own = pltpu.make_async_copy(parts_ref.at[me], hold, own_sems.at[0])
+    own.start()
+    own.wait()
+    own = pltpu.make_async_copy(hold, out_ref.at[me], own_sems.at[1])
+    own.start()
+    own.wait()
+    for k in range(1, group):
+        copy = across(k, (me + group - k) % group)
+        copy.wait_recv()
+        copy.wait_send()
+
+
+def return_parts(parts):
+    group = parts.shape[0]
+    return pl.pallas_call(
+        functools.partial(return_kernel, group),
+        out_shape=jax.ShapeDtypeStruct(parts.shape, parts.dtype),
+        in_specs=[pl.BlockSpec(memory_space=pl.ANY)],
+        out_specs=pl.BlockSpec(memory_space=pl.ANY),
+        scratch_shapes=[
+            pltpu.VMEM(parts.shape[1:], parts.dtype),
+            pltpu.SemaphoreType.DMA((2, group)),
+            pltpu.SemaphoreType.DMA((2,)),
+        ],
+        compiler_params=pltpu.CompilerParams(collective_id=2, has_side_effects=True),
+    )(parts)
+
+
 def local(
     residual,
     queries_narrow,
@@ -73,6 +341,7 @@
     down_weight,
 ):
     local_count = queries_narrow.shape[0]
+    up_full, down_full = share_weights(up_weight, down_weight)
     table_narrow, table_broad = (
         lax.all_gather(gates_narrow, "sp", axis=0, tiled=True),
         lax.all_gather(gates_broad, "sp", axis=0, tiled=True),
@@ -121,21 +390,22 @@
         tiled=True,
     ).astype(jnp.float32)
     mixed = (residual.astype(jnp.float32) + projected).astype(jnp.bfloat16)
-    features = lax.all_gather(rms_scaled(mixed, norm_gain), "tp", axis=0, tiled=True)
+    features = gather_rows(rms_scaled(mixed, norm_gain))
+    tp_count, group, rows, width = features.shape
     up_total = jnp.dot(
-        features,
-        lax.all_gather(up_weight, "sp", axis=0, tiled=True),
+        features.reshape(tp_count * group * rows, width),
+        up_full,
         preferred_element_type=jnp.float32,
     )
     hidden = jnp.square(jax.nn.relu(up_total)).astype(jnp.bfloat16)
-    down_term = jnp.dot(
-        hidden,
-        lax.all_gather(down_weight, "sp", axis=1, tiled=True),
-        preferred_element_type=jnp.float32,
-    )
-    summed_rows = lax.psum_scatter(
-        down_term.astype(jnp.bfloat16), "tp", scatter_dimension=0, tiled=True
-    ).astype(jnp.float32)
+    down_term = jnp.dot(hidden, down_full, preferred_element_type=jnp.float32)
+    parts = lax.psum_scatter(
+        down_term.astype(jnp.bfloat16).reshape(features.shape),
+        "tp",
+        scatter_dimension=0,
+        tiled=False,
+    )
+    summed_rows = jnp.sum(return_parts(parts).astype(jnp.float32), axis=0)
     return (mixed.astype(jnp.float32) + summed_rows).astype(jnp.bfloat16)
 
 

time: 743 us -> 506 us (0.68)
  waiting for transfers between devices: 557 us -> 124 us
  Pallas kernels: 0 us -> 200 us
    all_gather x2 -> x0, waiting for transfers between devices: 440 us -> none  [the longest x1 250 us: local(): lax.all_gather(down_weight, 'sp', axis=1, tiled=True)]
    pallas_call x0 -> x3, Pallas kernels: none -> 200 us  [the longest x1 81.6 us: gather_rows(): pl.pallas_call(functools.partial(gather_kernel, group, tp_count), out_sha...]
    reduce_scatter x1, waiting for transfers between devices: 6.5 us -> 20.9 us  [local(): lax.psum_scatter(down_term.astype(jnp.bfloat16).reshape(features.shape),...]
  transfers between devices with their start and end apart: 8 -> 6, of which waited for: 7 -> 4; matrix products, arithmetic and copies ran while one was open for 7% -> 10% of each run, Pallas kernels for 0% -> 14%
where the time goes in v1:
time: 506 us; the launch traced here: 505 us
  Pallas kernels  200 us (40%)
  waiting for transfers between devices  124 us (25%)
  blocking collectives  79.8 us (16%)
  matrix products  46.6 us (9%)
  local copies, waits for them, and re-layouts  21.4 us (4%)
  other arithmetic  19.2 us (4%)
  between operations  13.7 us (3%)
    pallas_call x1, Pallas kernels, gather_rows(): pl.pallas_call(functools.partial(gather_kernel, group, tp_count), out_sha...  81.6 us
    pallas_call x1, Pallas kernels, share_weights(): pl.pallas_call(functools.partial(weights_kernel, count, group), out_shape...  69.4 us
    pallas_call x1, Pallas kernels, return_parts(): pl.pallas_call(functools.partial(return_kernel, group), out_shape=jax.Sha...  49 us
    all_gather x1, waiting for transfers between devices, local(): lax.all_gather(values_narrow, 'sp', axis=0, tiled=True)  48.3 us
    all_gather x1, blocking collectives, local(): lax.all_gather(gates_narrow, 'sp', axis=0, tiled=True)  43.5 us
    all_gather x1, waiting for transfers between devices, local(): piece_values_broad = lax.all_gather(values_broad, 'sp', axis=0, tiled=True)  42.1 us
    all_gather x1, blocking collectives, local(): lax.all_gather(gates_broad, 'sp', axis=0, tiled=True)  36.3 us
    reduce_scatter x1, waiting for transfers between devices, local(): lax.psum_scatter(down_term.astype(jnp.bfloat16).reshape(features.shape),...  20.9 us
  transfers between devices with their start and end apart: 6, of which 4 were waited for; matrix products, arithmetic and copies ran while one was open for 10% of the time, Pallas kernels for 14%

profile of v1, /device:TPU:0, one launch (start us, length us, event | category | flops | bytes accessed | tf_op | source)
XLA Modules:
  0.0 505.2 jit_solution(8246214581181659811)
XLA Ops:
  6.5 0.7 all-gather.7.cloned.1.call-update
  7.3 0.0 all-gather.11.cloned.1.call-start
  7.3 0.7 all-gather.11.cloned.1.call-update
  8.0 0.0 all-gather.9.cloned.1.call-start
  8.1 0.7 all-gather.9.cloned.1.call-update
  8.7 0.0 all-gather.13.cloned.1.call-start
  8.8 0.5 all-gather.13.cloned.1.call-update
  9.3 0.0 reduce-scatter.3.cloned.1.call-start
  9.4 1.3 iota_compare_fusion
  10.7 43.5 %all-gather = f32[16,192,8]{1,2,0:T(8,128)S(1)} all-gather(f32[1,192,8]{1,2,0:T(8,128)} %bitcast.65), channel_id=1, replica_groups=mesh['sp'=16,'tp'=2] {'sp'}, dimensions={0}, use_global_device_ids=true | all-gather | bytes 104448 | tf_op jit(solution)/shard_map/all_gather | solution.py:346
  54.3 0.7 reshape.100
  55.0 1.7 copy.29
  56.7 36.3 %all-gather.1 = f32[16,192,4]{1,2,0:T(4,128)S(1)} all-gather(f32[1,192,4]{1,2,0:T(4,128)} %bitcast.71), channel_id=1, replica_groups=mesh['sp'=16,'tp'=2] {'sp'}, dimensions={0}, use_global_device_ids=true | all-gather | bytes 52224 | tf_op jit(solution)/shard_map/all_gather | solution.py:347
  93.0 0.1 reshape.102
  93.1 1.6 copy.33
  94.8 2.6 copy.30
  97.4 7.4 %fusion.2 = (f32[8,192]{1,0:T(8,128)S(1)}, f32[8,192,3072]{2,1,0:T(8,128)S(1)}) fusion(f32[8,3072]{1,0:T(8,128)} %bitcast.58, f32[8,192]{1,0:T(8,128)} %bitcast.66, pred[192,3072]{1,0:T(8,128)(4,1)} %get-tuple-element.9, bf16[192,8,32]{0,2,1:T(8,128)(2,1)} %bitcast.62, bf16[3072,8,32]{0,2,1:T(8,128)(2,1)} %bitcast.56), kind=kOutput, calls=%fused_computation.4 | convolution fusion | flops 325581312 | bytes 21245952 | tf_op jit(solution)/shard_map/qhd,khd->hqk/dot_general | solution.py:19
  104.8 0.0 copy-start.10
  104.8 6.4 %copy-done.2 = f32[8,192,3072]{2,1,0:T(8,128)} copy-done((f32[8,192,3072]{2,1,0:T(8,128)}, f32[8,192,3072]{2,1,0:T(8,128)S(1)}, u32[]{:S(2)}) %copy-start.2) | copy-done | bytes 18874392
  111.2 0.3 copy-done.10
  111.6 8.6 %fusion = f32[8,192]{1,0:T(8,128)} fusion(f32[8,192,3072]{2,1,0:T(8,128)S(1)} %get-tuple-element.12, f32[192,3072]{1,0:T(8,128)S(1)} %get-tuple-element.10, f32[8,192]{1,0:T(8,128)S(1)} %broadcast_maximum_fusion, f32[8,3072]{1,0:T(8,128)S(1)} %bitcast.59, f32[8,192]{1,0:T(8,128)S(1)} %bitcast.68, pred[192,3072]{1,0:T(8,128)(4,1)S(1)} %copy-done.6), kind=kLoop, calls=%fused_computation.2 | loop fusion | flops 33028608 | bytes 21940224 | tf_op jit(solution)/shard_map/reduce_sum | solution.py:29
  120.2 10.3 %all-gather.11.cloned.1.call-done = bf16[3072,256]{1,0:T(8,128)(2,1)} async-done(((bf16[192,256]{1,0:T(8,128)(2,1)}), bf16[3072,256]{1,0:T(8,128)(2,1)}) %all-gather.11.cloned.1.call-update) | async-done | bytes 1572880 | tf_op jit(solution)/shard_map/all_gather | solution.py:356
  130.5 2.6 copy.34
  133.1 8.5 %fusion.41 = (f32[4,192]{1,0:T(4,128)}, f32[4,192,3072]{2,1,0:T(8,128)}) fusion(f32[4,3072]{1,0:T(4,128)S(1)} %bitcast.64, f32[4,192]{1,0:T(4,128)} %bitcast.72, bf16[192,4,64]{0,2,1:T(8,128)(2,1)} %bitcast.61, bf16[3072,4,64]{0,2,1:T(8,128)(2,1)} %bitcast.55, pred[192,3072]{1,0:T(8,128)(4,1)} %get-tuple-element.9), kind=kOutput, calls=%fused_computation.44 | convolution fusion | flops 313785600 | bytes 11753472 | tf_op jit(solution)/shard_map/qhd,khd->hqk/dot_general | solution.py:19
  141.7 48.3 %all-gather.9.cloned.1.call-done = bf16[3072,256]{1,0:T(8,128)(2,1)} async-done(((bf16[192,256]{1,0:T(8,128)(2,1)}), bf16[3072,256]{1,0:T(8,128)(2,1)}) %all-gather.9.cloned.1.call-update) | async-done | bytes 1572880 | tf_op jit(solution)/shard_map/all_gather | solution.py:355
  190.0 2.6 copy.32
  192.6 0.7 broadcast_maximum_fusion.1
  193.3 10.5 %fusion.24 = bf16[192,8,32]{0,2,1:T(8,128)(2,1)S(1)} fusion(bf16[3072,8,32]{0,2,1:T(8,128)(2,1)} %bitcast.54, f32[8,192,3072]{2,1,0:T(8,128)} %copy-done.2, f32[192,3072]{1,0:T(8,128)S(1)} %get-tuple-element.10, f32[8,192]{1,0:T(8,128)} %copy-done.10, f32[8,3072]{1,0:T(8,128)S(1)} %bitcast.60, f32[8,192]{1,0:T(8,128)} %bitcast.67, ...), kind=kOutput, calls=%fused_computation.28 | convolution fusion | flops 335118336 | bytes 23611392 | tf_op jit(solution)/shard_map/hqk,khd->hqd/dot_general | solution.py:30
  203.8 1.6 fusion.42
  205.4 1.8 fusion.6
  207.2 42.1 %all-gather.13.cloned.1.call-done = bf16[3072,256]{1,0:T(8,128)(2,1)} async-done(((bf16[192,256]{1,0:T(8,128)(2,1)}), bf16[3072,256]{1,0:T(8,128)(2,1)}) %all-gather.13.cloned.1.call-update) | async-done | bytes 1572880 | tf_op jit(solution)/shard_map/all_gather | solution.py:357
  249.3 2.6 copy.36
  251.9 6.1 %fusion.30 = bf16[192,4,64]{0,2,1:T(8,128)(2,1)S(1)} fusion(bf16[3072,4,64]{0,2,1:T(8,128)(2,1)} %bitcast.52, f32[4,192,3072]{2,1,0:T(8,128)} %get-tuple-element.14, f32[192,3072]{1,0:T(8,128)S(1)} %get-tuple-element.10, f32[4,192]{1,0:T(4,128)S(1)} %broadcast_maximum_fusion.1, f32[192,4]{0,1:T(4,128)S(1)} %bitcast.69), kind=kOutput, calls=%fused_computation.30 | convolution fusion | flops 309166080 | bytes 13473792 | tf_op jit(solution)/shard_map/hqk,khd->hqd/dot_general | solution.py:30
  258.1 1.4 fusion.14
  259.5 0.0 reduce-scatter.3.cloned.1.call-update
  259.5 0.0 reduce-scatter.5.cloned.1.call-start
  259.5 69.4 %shard_map.137 = (bf16[2048,512]{1,0:T(8,128)(2,1)}, bf16[512,2048]{1,0:T(8,128)(2,1)}) custom-call(bf16[128,4096]{1,0:T(8,128)(2,1)} %up_ref.1, bf16[4096,128]{1,0:T(8,128)(2,1)} %down_ref.1), custom_call_target="tpu_custom_call" | custom-call | bytes 83886080 | tf_op jit(solution)/shard_map/pallas_call | solution.py:163
  329.0 0.0 reduce-scatter.3.cloned.1.call-done
  329.0 1.4 fusion.33
  330.4 1.9 fusion.35.rows_ref
  332.3 81.6 %shard_map.136 = bf16[2,8,96,2048]{3,2,1,0:T(8,128)(2,1)} custom-call(bf16[96,2048]{1,0:T(8,128)(2,1)} %fusion.35.rows_ref), custom_call_target="tpu_custom_call" | custom-call | tf_op jit(solution)/shard_map/pallas_call | solution.py:257
  413.9 11.1 %convolution_convert_fusion = bf16[1536,2048]{1,0:T(8,128)(2,1)} fusion(bf16[512,2048]{1,0:T(8,128)(2,1)} %get-tuple-element.8, bf16[1536,2048]{1,0:T(8,128)(2,1)} %bitcast.51, bf16[2048,512]{1,0:T(8,128)(2,1)S(1)} %copy-done.12), kind=kOutput, calls=%fused_computation.11 | convolution fusion | flops 6447955968 | bytes 16777216 | tf_op jit(solution)/shard_map/dot_general | solution.py:401
  425.0 0.0 reduce-scatter.5.cloned.1.call-update
  425.0 0.0 copy-start.1
  425.0 20.9 %reduce-scatter.5.cloned.1.call-done = bf16[1,8,96,2048]{3,2,1,0:T(8,128)(2,1)} async-done(((bf16[2,8,96,2048]{3,2,1,0:T(8,128)(2,1)}), bf16[1,8,96,2048]{3,2,1,0:T(8,128)(2,1)}) %reduce-scatter.5.cloned.1.call-update) | async-done | bytes 3145744 | tf_op jit(solution)/shard_map/reduce_scatter | solution.py:402
  445.9 49.0 %shard_map.138 = bf16[8,96,2048]{2,1,0:T(8,128)(2,1)} custom-call(bf16[8,96,2048]{2,1,0:T(8,128)(2,1)} %bitcast.53), custom_call_target="tpu_custom_call" | custom-call | tf_op jit(solution)/shard_map/pallas_call | solution.py:313
  494.9 2.5 convert_reduce_fusion
  497.4 0.9 fusion.36
  (36 shorter events, 0.1 us)
Async XLA Ops:
  6.5 197.3 %copy-start = (bf16[256,2048]{1,0:T(8,128)(2,1)S(1)}, bf16[256,2048]{1,0:T(8,128)(2,1)}, u32[]{:S(2)}) copy-start(bf16[256,2048]{1,0:T(8,128)(2,1)} %param.23) | copy-start | bytes 3145732
  6.5 88.2 %all-gather.7.cloned.1.call-start = ((), (), s32[]{:S(2)}) async-start(), calls=%async_computation.2 | async-start | bytes 1671168 | tf_op jit(solution)/shard_map/all_gather | solution.py:354
  7.3 123.3 %all-gather.11.cloned.1.call-start = ((), (), s32[]{:S(2)}) async-start(), calls=%async_computation.4 | async-start | bytes 1671168 | tf_op jit(solution)/shard_map/all_gather | solution.py:356
  8.0 182.0 %all-gather.9.cloned.1.call-start = ((), (), s32[]{:S(2)}) async-start(), calls=%async_computation.3 | async-start | bytes 1671168 | tf_op jit(solution)/shard_map/all_gather | solution.py:355
  8.7 240.6 %all-gather.13.cloned.1.call-start = ((), (), s32[]{:S(2)}) async-start(), calls=%async_computation.5 | async-start | bytes 1671168 | tf_op jit(solution)/shard_map/all_gather | solution.py:357
  9.3 319.7 %reduce-scatter.3.cloned.1.call-start = ((), (), s32[]{:S(2)}) async-start(), calls=%async_computation.6 | async-start | bytes 1179648 | tf_op jit(solution)/shard_map/reduce_scatter | solution.py:383
  97.3 14.2 %copy-start.6 = (pred[192,3072]{1,0:T(8,128)(4,1)S(1)}, pred[192,3072]{1,0:T(8,128)(4,1)}, u32[]{:S(2)}) copy-start(pred[192,3072]{1,0:T(8,128)(4,1)} %get-tuple-element.9) | copy-start | bytes 1769476
  97.3 14.2 %copy-start.8 = (f32[3072,8]{0,1:T(8,128)S(1)}, f32[3072,8]{0,1:T(8,128)}, u32[]{:S(2)}) copy-start(f32[3072,8]{0,1:T(8,128)} %reshape.100) | copy-start | bytes 294916
  97.3 14.2 %copy-start.9 = (f32[192,8]{0,1:T(8,128)S(1)}, f32[192,8]{0,1:T(8,128)}, u32[]{:S(2)}) copy-start(f32[192,8]{0,1:T(8,128)} %param.21) | copy-start | bytes 18436
  104.8 6.5 %copy-start.2 = (f32[8,192,3072]{2,1,0:T(8,128)}, f32[8,192,3072]{2,1,0:T(8,128)S(1)}, u32[]{:S(2)}) copy-start(f32[8,192,3072]{2,1,0:T(8,128)S(1)} %get-tuple-element.12) | copy-start | bytes 56623108
  104.8 6.8 %copy-start.10 = (f32[8,192]{1,0:T(8,128)}, f32[8,192]{1,0:T(8,128)S(1)}, u32[]{:S(2)}) copy-start(f32[8,192]{1,0:T(8,128)S(1)} %broadcast_maximum_fusion) | copy-start | bytes 18436
  193.3 12.1 %slice-start = ((s8[9437184]{0:T(1024)(128)(4,1)}), s8[4194304]{0:T(1024)(128)(4,1)S(1)}, s32[]{:S(2)}) async-start(s8[9437184]{0:T(1024)(128)(4,1)} %bitcast.48), calls=%async_computation.8 | async-start | bytes 8388608
  193.3 12.1 %slice-start.1 = ((s8[9437184]{0:T(1024)(128)(4,1)}), s8[4194304]{0:T(1024)(128)(4,1)S(1)}, s32[]{:S(2)}) async-start(s8[9437184]{0:T(1024)(128)(4,1)} %bitcast.48), calls=%async_computation.9 | async-start | bytes 8388608
  193.3 12.1 %slice-start.2 = ((s8[9437184]{0:T(1024)(128)(4,1)}), s8[1048576]{0:T(1024)(128)(4,1)S(1)}, s32[]{:S(2)}) async-start(s8[9437184]{0:T(1024)(128)(4,1)} %bitcast.48), calls=%async_computation.10 | async-start | bytes 2097152
  251.9 6.2 %copy-start.3 = (f32[192,2048]{1,0:T(8,128)S(1)}, f32[192,2048]{1,0:T(8,128)}, u32[]{:S(2)}) copy-start(f32[192,2048]{1,0:T(8,128)} %fusion.42) | copy-start | bytes 4718596
  251.9 6.2 %copy-start.7 = (bf16[256,2048]{1,0:T(8,128)(2,1)S(1)}, bf16[256,2048]{1,0:T(8,128)(2,1)}, u32[]{:S(2)}) copy-start(bf16[256,2048]{1,0:T(8,128)(2,1)} %param.24) | copy-start | bytes 3145732
  258.0 71.0 %copy-start.4 = (bf16[96,2048]{1,0:T(8,128)(2,1)S(1)}, bf16[96,2048]{1,0:T(8,128)(2,1)}, u32[]{:S(2)}) copy-start(bf16[96,2048]{1,0:T(8,128)(2,1)} %param.14) | copy-start | bytes 1179652
  258.1 72.3 %copy-start.11 = (f32[2048]{0:T(1024)S(1)}, f32[2048]{0:T(1024)}, u32[]{:S(2)}) copy-start(f32[2048]{0:T(1024)} %param.25) | copy-start | bytes 24580
  259.5 186.4 %reduce-scatter.5.cloned.1.call-start = ((), (), s32[]{:S(2)}) async-start(), calls=%async_computation.7 | async-start | bytes 9437184 | tf_op jit(solution)/shard_map/reduce_scatter | solution.py:402
  329.0 84.9 %copy-start.12 = (bf16[2048,512]{1,0:T(8,128)(2,1)S(1)}, bf16[2048,512]{1,0:T(8,128)(2,1)}, u32[]{:S(2)}) copy-start(bf16[2048,512]{1,0:T(8,128)(2,1)} %get-tuple-element.7) | copy-start | bytes 6291460
  425.0 72.4 %copy-start.5 = (bf16[96,2048]{1,0:T(8,128)(2,1)S(1)}, bf16[96,2048]{1,0:T(8,128)(2,1)}, u32[]{:S(2)}) copy-start(bf16[96,2048]{1,0:T(8,128)(2,1)} %reduce-scatter.3.cloned.1.call-done) | copy-start | bytes 1179652
  425.0 73.3 %copy-start.1 = (bf16[256,2048]{1,0:T(8,128)(2,1)S(1)}, bf16[256,2048]{1,0:T(8,128)(2,1)}, u32[]{:S(2)}) copy-start(bf16[256,2048]{1,0:T(8,128)(2,1)} %param.23) | copy-start | bytes 3145732
Sparse Core Ops, SparseCore 0:
  10.1 60.9 all-gather.6
  73.8 56.6 all-gather.10
  133.3 56.6 all-gather.8
  192.6 56.6 all-gather.12
  259.6 6.8 reduce-scatter.2
  425.1 20.7 reduce-scatter.4

commit v2 on v1

--- a/solution.py
+++ b/solution.py
@@ -11,49 +11,6 @@
 B_DIM = 64
 
 
-def group_update(state, queries, keys, values, query_gates, key_gates, allowed, head_size):
-    peak, total, summed = state
-    query_count = queries.shape[0]
-    key_count = keys.shape[0]
-    heads = queries.shape[1] // head_size
-    scores = jnp.einsum(
-        "qhd,khd->hqk",
-        queries.reshape(query_count, heads, head_size),
-        keys.reshape(key_count, heads, head_size),
-        preferred_element_type=jnp.float32,
-    ) * head_size ** (-0.5)
-    scores = scores + query_gates.T[:, :, None] - key_gates.T[:, None, :]
-    scores = jnp.where(allowed[None], scores, -1e30)
-    new_peak = jnp.maximum(peak, jnp.max(scores, axis=-1))
-    weights = jnp.exp(scores - new_peak[..., None]) * allowed[None].astype(jnp.float32)
-    total = jnp.sum(weights, axis=-1)
-    summed = jnp.einsum(
-        "hqk,khd->hqd",
-        weights.astype(jnp.bfloat16),
-        values.reshape(key_count, heads, head_size),
-        preferred_element_type=jnp.float32,
-    )
-    return (new_peak, total, summed)
-
-
-def empty_state(query_count, heads, head_size):
-    return (
-        jnp.full((heads, query_count), -1e30, jnp.float32),
-        jnp.zeros((heads, query_count), jnp.float32),
-        jnp.zeros((heads, query_count, head_size), jnp.float32),
-    )
-
-
-def finish_group(state, head_size):
-    peak, total, summed = state
-    result = summed / total[..., None]
-    return (
-        result.transpose(1, 0, 2)
-        .reshape(result.shape[1], result.shape[0] * head_size)
-        .astype(jnp.bfloat16)
-    )
-
-
 def rms_scaled(mixed, norm_gain):
     mixed_wide = mixed.astype(jnp.float32)
     scale = lax.rsqrt(jnp.mean(mixed_wide * mixed_wide, axis=-1, keepdims=True) + 1e-06)
@@ -64,10 +21,114 @@
     return 8 if sp_count % 8 == 0 else sp_count
 
 
-def weights_kernel(
-    count, group, up_ref, down_ref, up_out, down_out, up_hold, down_hold, sems, own_sems
+def head_columns(narrow_heads):
+    ranges = [(h * A_DIM, (h + 1) * A_DIM, A_DIM) for h in range(narrow_heads)]
+    return ranges + [(narrow_heads * A_DIM, narrow_heads * A_DIM + B_DIM, B_DIM)]
+
+
+def attend_block(ranges, block, query, kv_all, gate_all):
+    tokens, width = query.shape
+    lane = lax.broadcasted_iota(jnp.int32, (tokens, width), 1)
+    row = lax.broadcasted_iota(jnp.int32, (tokens, tokens), 0)
+    column = lax.broadcasted_iota(jnp.int32, (tokens, tokens), 1)
+    inside = [(lane >= low) & (lane < high) for low, high, _ in ranges]
+    wide = query.astype(jnp.float32)
+    head_queries = [jnp.where(mask, wide, 0.0).astype(jnp.bfloat16) for mask in inside]
+    own_gates = gate_all[block]
+    query_gates = [
+        jnp.sum(jnp.where(row == column, own_gates[h : h + 1, :], 0.0), axis=1, keepdims=True)
+        for h in range(len(ranges))
+    ]
+
+    def by_head(columns):
+        spread = jnp.broadcast_to(columns[-1], (tokens, width))
+        for mask, values in zip(inside[:-1], columns[:-1]):
+            spread = jnp.where(mask, values, spread)
+        return spread
+
+    def step(key_block, state):
+        peaks, totals, summed = state
+        keys = kv_all[key_block, :, :width]
+        values = kv_all[key_block, :, width:]
+        key_gates = gate_all[key_block]
+        allowed = column + (key_block - block) * tokens <= row
+        new_peaks, new_totals, fades, terms = [], [], [], []
+        for h, (_, _, size) in enumerate(ranges):
+            scores = (
+                lax.dot_general(
+                    head_queries[h],
+                    keys,
+                    (((1,), (1,)), ((), ())),
+                    preferred_element_type=jnp.float32,
+                )
+                * size ** (-0.5)
+                + query_gates[h]
+                - key_gates[h : h + 1, :]
+            )
+            scores = jnp.where(allowed, scores, -1e30)
+            peak = jnp.maximum(peaks[h], jnp.max(scores, axis=1, keepdims=True))
+            weights = jnp.exp(scores - peak)
+            fade = jnp.exp(peaks[h] - peak)
+            new_peaks.append(peak)
+            new_totals.append(totals[h] * fade + jnp.sum(weights, axis=1, keepdims=True))
+            fades.append(fade)
+            terms.append(
+                jnp.dot(
+                    weights.astype(jnp.bfloat16), values, preferred_element_type=jnp.float32
+                )
+            )
+        summed = summed * by_head(fades) + by_head(terms)
+        return tuple(new_peaks), tuple(new_totals), summed
+
+    heads = len(ranges)
+    initial = (
+        tuple(jnp.full((tokens, 1), -1e30, jnp.float32) for _ in range(heads)),
+        tuple(jnp.zeros((tokens, 1), jnp.float32) for _ in range(heads)),
+        jnp.zeros((tokens, width), jnp.float32),
+    )
+    _, totals, summed = lax.fori_loop(0, block + 1, step, initial)
+    return (summed / by_head(totals)).astype(jnp.bfloat16)
+
+
+def layer_kernel(
+    count,
+    group,
+    ranges,
+    q_ref,
+    kv_ref,
+    gate_ref,
+    up_ref,
+    down_ref,
+    attended_out,
+    up_out,
+    down_out,
+    q_all,
+    kv_all,
+    gate_all,
+    attended,
+    up_hold,
+    down_hold,
+    kv_sems,
+    gate_sems,
+    q_sems,
+    back_sems,
+    sems,
+    own_sems,
 ):
     me = lax.axis_index("sp")
+    head_groups = q_ref.shape[0]
+    parts = count // head_groups
+    my_heads = me % head_groups
+    my_part = me // head_groups
+
+    def block_of(part, slot):
+        turn = slot % 2
+        return slot * parts + (1 - turn) * part + turn * (parts - 1 - part)
+
+    my_slot = me // parts
+    my_turn = my_slot % 2
+    place = me % parts
+    reader_part = (1 - my_turn) * place + my_turn * (parts - 1 - place)
     up_rows = up_ref.shape[0]
     units = up_out.shape[1]
     columns = down_ref.shape[1]
@@ -84,6 +145,50 @@
 
     lax.fori_loop(1, count, hello, 0)
     pl.semaphore_wait(barrier, count - 1)
+
+    def remote(source, target, sem_pair, first, second, peer):
+        return pltpu.make_async_remote_copy(
+            src_ref=source,
+            dst_ref=target,
+            send_sem=sem_pair.at[0, first],
+            recv_sem=sem_pair.at[1, second],
+            device_id={"sp": peer},
+            device_id_type=pl.DeviceIdType.MESH,
+        )
+
+    def context_copies(k, owner):
+        peer = (me + k) % count
+        heads = peer % head_groups
+        return (
+            remote(kv_ref.at[heads], kv_all.at[owner], kv_sems, k, k, peer),
+            remote(gate_ref.at[heads], gate_all.at[owner], gate_sems, k, k, peer),
+        )
+
+    def start_context(k, carry):
+        for copy in context_copies(k, me):
+            copy.start()
+        return carry
+
+    def wait_context(k, carry):
+        for copy in context_copies(k, (me + count - k) % count):
+            copy.wait_recv()
+            copy.wait_send()
+        return carry
+
+    for heads in range(head_groups):
+        reader = reader_part * head_groups + heads
+
+        @pl.when(reader != me)
+        def _():
+            remote(q_ref.at[heads], q_all.at[my_slot], q_sems, heads, my_slot, reader).start()
+
+        @pl.when(reader == me)
+        def _():
+            q_all[my_slot] = q_ref[heads]
+
+    lax.fori_loop(1, count, start_context, 0)
+    kv_all[me] = kv_ref[my_heads]
+    gate_all[me] = gate_ref[my_heads]
 
     def up_source(chunk):
         return up_ref.at[:, pl.ds(pl.multiple_of(chunk * units, 128), units)]
@@ -145,12 +250,65 @@
     ]
     for copy in second:
         copy.start()
+    for heads in range(head_groups):
+        reader = reader_part * head_groups + heads
+
+        @pl.when(reader != me)
+        def _():
+            remote(q_ref.at[heads], q_all.at[my_slot], q_sems, heads, my_slot, reader).wait_send()
+
+    for slot in range(head_groups):
+        owner = block_of(my_part, slot)
+
+        @pl.when(owner != me)
+        def _():
+            remote(q_ref.at[0], q_all.at[slot], q_sems, 0, slot, owner).wait_recv()
+
+    lax.fori_loop(1, count, wait_context, 0)
+
+    def attend(slot, carry):
+        block = block_of(my_part, slot)
+        attended[slot] = attend_block(ranges, block, q_all[slot], kv_all, gate_all)
+        return carry
+
+    lax.fori_loop(0, head_groups, attend, 0)
+    for slot in range(head_groups):
+        owner = block_of(my_part, slot)
+
+        @pl.when(owner != me)
+        def _():
+            remote(
+                attended.at[slot], attended_out.at[my_heads], back_sems, slot, my_heads, owner
+            ).start()
+
+        @pl.when(owner == me)
+        def _():
+            attended_out[my_heads] = attended[slot]
+
     for copy in second:
         copy.wait()
     lax.fori_loop(1, count, finish, 0)
-
-
-def share_weights(up_weight, down_weight):
+    for slot in range(head_groups):
+        owner = block_of(my_part, slot)
+
+        @pl.when(owner != me)
+        def _():
+            remote(
+                attended.at[slot], attended_out.at[my_heads], back_sems, slot, my_heads, owner
+            ).wait_send()
+
+    for heads in range(head_groups):
+        reader = reader_part * head_groups + heads
+
+        @pl.when(reader != me)
+        def _():
+            remote(
+                attended.at[0], attended_out.at[heads], back_sems, 0, heads, reader
+            ).wait_recv()
+
+
+def attend_and_share(queries, keys_values, gates, ranges, up_weight, down_weight):
+    head_groups, tokens, head_width = queries.shape
     count = lax.axis_size("sp")
     group = group_size(count)
     up_rows, unit_total = up_weight.shape
@@ -160,17 +318,28 @@
         down_shape = (units, count * columns)
     else:
         down_shape = (count, units, columns)
-    up_full, down_full = pl.pallas_call(
-        functools.partial(weights_kernel, count, group),
+    attended, up_full, down_full = pl.pallas_call(
+        functools.partial(layer_kernel, count, group, ranges),
         out_shape=(
+            jax.ShapeDtypeStruct(queries.shape, queries.dtype),
             jax.ShapeDtypeStruct((count * up_rows, units), up_weight.dtype),
             jax.ShapeDtypeStruct(down_shape, down_weight.dtype),
         ),
-        in_specs=[pl.BlockSpec(memory_space=pl.ANY)] * 2,
-        out_specs=[pl.BlockSpec(memory_space=pl.ANY)] * 2,
+        in_specs=[pl.BlockSpec(memory_space=pltpu.VMEM)] * 3
+        + [pl.BlockSpec(memory_space=pl.ANY)] * 2,
+        out_specs=[pl.BlockSpec(memory_space=pltpu.VMEM)]
+        + [pl.BlockSpec(memory_space=pl.ANY)] * 2,
         scratch_shapes=[
+            pltpu.VMEM(queries.shape, queries.dtype),
+            pltpu.VMEM((count,) + keys_values.shape[1:], keys_values.dtype),
+            pltpu.VMEM((count,) + gates.shape[1:], gates.dtype),
+            pltpu.VMEM(queries.shape, queries.dtype),
             pltpu.VMEM((up_rows, units), up_weight.dtype),
             pltpu.VMEM((units, columns), down_weight.dtype),
+            pltpu.SemaphoreType.DMA((2, count)),
+            pltpu.SemaphoreType.DMA((2, count)),
+            pltpu.SemaphoreType.DMA((2, head_groups)),
+            pltpu.SemaphoreType.DMA((2, head_groups)),
             pltpu.SemaphoreType.DMA((2, 2, count)),
             pltpu.SemaphoreType.DMA((2,)),
         ],
@@ -178,10 +347,10 @@
         cost_estimate=pl.CostEstimate(
             flops=0, bytes_accessed=count * up_rows * units * 80, transcendentals=0
         ),
-    )(up_weight, down_weight)
+    )(queries, keys_values, gates, up_weight, down_weight)
     if columns % 128:
         down_full = down_full.transpose(1, 0, 2).reshape(units, count * columns)
-    return up_full, down_full
+    return attended, up_full, down_full
 
 
 def gather_kernel(group, tp_count, rows_ref, out_ref, hold, sems, own_sems, pass_sems):
@@ -340,46 +509,34 @@
     up_weight,
     down_weight,
 ):
-    local_count = queries_narrow.shape[0]
-    up_full, down_full = share_weights(up_weight, down_weight)
-    table_narrow, table_broad = (
-        lax.all_gather(gates_narrow, "sp", axis=0, tiled=True),
-        lax.all_gather(gates_broad, "sp", axis=0, tiled=True),
+    tokens = queries_narrow.shape[0]
+    head_groups = gates_broad.shape[1]
+    narrow_heads = gates_narrow.shape[1] // head_groups
+    ranges = head_columns(narrow_heads)
+
+    def by_group(narrow, broad):
+        return jnp.concatenate(
+            [part.reshape(tokens, head_groups, -1) for part in (narrow, broad)], axis=-1
+        ).transpose(1, 0, 2)
+
+    gates = jnp.concatenate(
+        [gates_narrow.reshape(tokens, head_groups, narrow_heads), gates_broad[..., None]], axis=-1
+    ).transpose(1, 2, 0)
+    gates = jnp.pad(gates, ((0, 0), (0, -gates.shape[1] % 8), (0, 0)))
+    attended, up_full, down_full = attend_and_share(
+        by_group(queries_narrow, queries_broad),
+        jnp.concatenate(
+            [by_group(keys_narrow, keys_broad), by_group(values_narrow, values_broad)], axis=-1
+        ),
+        gates,
+        ranges,
+        up_weight,
+        down_weight,
     )
-    query_pos = lax.axis_index("sp") * local_count + jnp.arange(local_count, dtype=jnp.int32)
-    initial = (
-        empty_state(local_count, queries_narrow.shape[1] // A_DIM, A_DIM),
-        empty_state(local_count, queries_broad.shape[1] // B_DIM, B_DIM),
-    )
-    piece_keys_narrow = lax.all_gather(keys_narrow, "sp", axis=0, tiled=True)
-    piece_values_narrow = lax.all_gather(values_narrow, "sp", axis=0, tiled=True)
-    piece_keys_broad = lax.all_gather(keys_broad, "sp", axis=0, tiled=True)
-    piece_values_broad = lax.all_gather(values_broad, "sp", axis=0, tiled=True)
-    piece_count = piece_keys_narrow.shape[0]
-    key_pos = jnp.arange(piece_count, dtype=jnp.int32)
-    allowed = key_pos[None, :] <= query_pos[:, None]
-    state_narrow = group_update(
-        initial[0],
-        queries_narrow,
-        piece_keys_narrow,
-        piece_values_narrow,
-        gates_narrow,
-        table_narrow,
-        allowed,
-        A_DIM,
-    )
-    state_broad = group_update(
-        initial[1],
-        queries_broad,
-        piece_keys_broad,
-        piece_values_broad,
-        gates_broad,
-        table_broad,
-        allowed,
-        B_DIM,
-    )
-    attended_narrow = finish_group(state_narrow, A_DIM)
-    attended_broad = finish_group(state_broad, B_DIM)
+    rows_first = attended.transpose(1, 0, 2)
+    split = narrow_heads * A_DIM
+    attended_narrow = rows_first[..., :split].reshape(tokens, -1)
+    attended_broad = rows_first[..., split:].reshape(tokens, -1)
     projected = lax.psum_scatter(
         (
             jnp.dot(attended_narrow, project_narrow, preferred_element_type=jnp.float32)

time: 506 us -> 328 us (0.65)
  blocking collectives: 79.8 us -> 0 us
  waiting for transfers between devices: 124 us -> 57.8 us
  matrix products: 46.6 us -> 12.8 us
  Pallas kernels: 200 us -> 225 us
  local copies, waits for them, and re-layouts: 21.4 us -> 10.5 us
  other arithmetic: 19.2 us -> 8.42 us
    all_gather x4 -> x0, waiting for transfers between devices: 101 us -> none  [the longest x1 48.3 us: local(): lax.all_gather(values_narrow, 'sp', axis=0, tiled=True)]
    all_gather x2 -> x0, blocking collectives: 79.8 us -> none  [the longest x1 43.5 us: local(): lax.all_gather(gates_narrow, 'sp', axis=0, tiled=True)]
    pallas_call x1, Pallas kernels: 69.4 us -> 125 us  [attend_and_share(): pl.pallas_call(functools.partial(layer_kernel, count, group, ranges), out...]
    reduce_scatter x1, waiting for transfers between devices: 0.02 us -> 38 us  [local(): lax.psum_scatter((jnp.dot(attended_narrow, project_narrow, preferred_elem...]
    dot_general x4 -> x0, matrix products: 32.5 us -> none  [the longest x2 16.6 us: group_update(): jnp.einsum('hqk,khd->hqd', weights.astype(jnp.bfloat16), values.reshape(k...]
    pallas_call x1, Pallas kernels: 81.6 us -> 50.4 us  [gather_rows(): pl.pallas_call(functools.partial(gather_kernel, group, tp_count), out_sha...]
    reduce_sum x2 -> x0, other arithmetic: 10.5 us -> none  [group_update(): total = jnp.sum(weights, axis=-1)]
    all_gather x6 -> x0, local copies, waits for them, and re-layouts: 10.4 us -> none  [the longest x1 2.61 us: local(): piece_keys_broad = lax.all_gather(keys_broad, 'sp', axis=0, tiled=True)]
  transfers between devices with their start and end apart: 6 -> 2, of which waited for: 4 -> 2; matrix products, arithmetic and copies ran while one was open for 10% -> 0% of each run, Pallas kernels for 14% -> 0%
where the time goes in v2:
time: 328 us
  Pallas kernels  225 us (69%)
  waiting for transfers between devices  57.8 us (18%)
  between operations  13.6 us (4%)
  matrix products  12.8 us (4%)
  local copies, waits for them, and re-layouts  10.5 us (3%)
  other arithmetic  8.42 us (3%)
    pallas_call x1, Pallas kernels, attend_and_share(): pl.pallas_call(functools.partial(layer_kernel, count, group, ranges), out...  125 us
    pallas_call x1, Pallas kernels, gather_rows(): pl.pallas_call(functools.partial(gather_kernel, group, tp_count), out_sha...  50.4 us
    pallas_call x1, Pallas kernels, return_parts(): pl.pallas_call(functools.partial(return_kernel, group), out_shape=jax.Sha...  49 us
    reduce_scatter x1, waiting for transfers between devices, local(): lax.psum_scatter((jnp.dot(attended_narrow, project_narrow, preferred_elem...  38 us
    reduce_scatter x1, waiting for transfers between devices, local(): lax.psum_scatter(down_term.astype(jnp.bfloat16).reshape(features.shape),...  19.8 us
    dot_general x1, matrix products, local(): down_term = jnp.dot(hidden, down_full, preferred_element_type=jnp.float32)  11.1 us
  transfers between devices with their start and end apart: 2, of which 2 were waited for; matrix products, arithmetic and copies ran while one was open for 0% of the time, Pallas kernels for 0%

profile of v2, /device:TPU:0, one launch (start us, length us, event | category | flops | bytes accessed | tf_op | source)
XLA Modules:
  0.0 327.7 jit_solution(5625753208808115502)
XLA Ops:
  6.5 0.0 copy-start
  6.5 0.0 reduce-scatter.3.cloned.1.call-start
  6.5 0.8 broadcast_in_dim.2
  7.3 0.7 reshape.48
  8.0 1.0 copy.15
  9.0 0.2 copy.17
  9.2 1.0 copy.19
  10.2 0.2 copy.21
  10.4 1.0 copy.23
  11.4 0.2 copy.25
  11.5 1.0 copy.16
  12.5 0.2 copy.18
  12.7 1.0 copy.20
  13.7 0.2 copy.22
  13.9 1.0 copy.24
  14.9 0.2 copy.26
  15.1 0.6 pad.4.gate_ref
  15.7 0.8 maximum_bitcast_fusion.q_ref
  16.5 0.2 maximum_bitcast_fusion.1
  16.7 0.8 pad_maximum_fusion.kv_ref
  17.5 0.0 copy-start.3
  17.5 125.1 %shard_map.136 = (bf16[4,192,128]{2,1,0:T(8,128)(2,1)}, bf16[2048,512]{1,0:T(8,128)(2,1)}, bf16[512,2048]{1,0:T(8,128)(2,1)}) custom-call(bf16[4,192,128]{2,1,0:T(8,128)(2,1)} %maximum_bitcast_fusion.q_ref, bf16[4,192,256]{2,1,0:T(8,128)(2,1)} %pad_maximum_fusion.kv_ref, f32[4,8,192]{2,1,0:T(8,128)} %pad.4.gate_ref, bf16[128,4096]{1,0:T(8,128)(2,1)} %up_ref.1, ...), custom_call_target="tpu_custom_call" | custom-call | bytes 83886080 | tf_op jit(solution)/shard_map/pallas_call | solution.py:321
  142.6 1.1 fusion.8
  143.7 0.1 copy.28
  143.9 0.1 copy.27
  144.0 0.0 copy-done
  144.0 0.0 copy-start.1
  144.0 0.4 fusion.9
  144.4 0.0 copy-start.4
  144.4 0.0 copy-done.3
  144.4 1.3 fusion.2
  145.8 0.0 reduce-scatter.3.cloned.1.call-update
  145.8 0.0 reduce-scatter.5.cloned.1.call-start
  145.9 38.0 %reduce-scatter.3.cloned.1.call-done = bf16[96,2048]{1,0:T(8,128)(2,1)} async-done(((bf16[192,2048]{1,0:T(8,128)(2,1)}), bf16[96,2048]{1,0:T(8,128)(2,1)}) %reduce-scatter.3.cloned.1.call-update) | async-done | bytes 393232 | tf_op jit(solution)/shard_map/reduce_scatter | solution.py:540
  183.9 0.0 copy-done.1
  183.9 1.2 fusion.3
  185.1 0.0 copy-done.4
  185.1 1.9 fusion.5.rows_ref
  187.0 50.4 %shard_map.137 = bf16[2,8,96,2048]{3,2,1,0:T(8,128)(2,1)} custom-call(bf16[96,2048]{1,0:T(8,128)(2,1)} %fusion.5.rows_ref), custom_call_target="tpu_custom_call" | custom-call | tf_op jit(solution)/shard_map/pallas_call | solution.py:426
  237.5 0.0 copy-done.5
  237.5 11.1 %convolution_convert_fusion = bf16[1536,2048]{1,0:T(8,128)(2,1)} fusion(bf16[512,2048]{1,0:T(8,128)(2,1)} %get-tuple-element.10, bf16[1536,2048]{1,0:T(8,128)(2,1)} %bitcast.32, bf16[2048,512]{1,0:T(8,128)(2,1)S(1)} %copy-done.5), kind=kOutput, calls=%fused_computation | convolution fusion | flops 6447955968 | bytes 16777216 | tf_op jit(solution)/shard_map/dot_general | solution.py:558
  248.5 0.0 reduce-scatter.5.cloned.1.call-update
  248.6 19.8 %reduce-scatter.5.cloned.1.call-done = bf16[1,8,96,2048]{3,2,1,0:T(8,128)(2,1)} async-done(((bf16[2,8,96,2048]{3,2,1,0:T(8,128)(2,1)}), bf16[1,8,96,2048]{3,2,1,0:T(8,128)(2,1)}) %reduce-scatter.5.cloned.1.call-update) | async-done | bytes 3145744 | tf_op jit(solution)/shard_map/reduce_scatter | solution.py:559
  268.3 49.0 %shard_map.138 = bf16[8,96,2048]{2,1,0:T(8,128)(2,1)} custom-call(bf16[8,96,2048]{2,1,0:T(8,128)(2,1)} %bitcast.33), custom_call_target="tpu_custom_call" | custom-call | tf_op jit(solution)/shard_map/pallas_call | solution.py:482
  317.3 0.0 copy-start.2
  317.4 2.6 convert_reduce_fusion
  319.9 0.0 copy-done.2
  320.0 0.9 fusion.6
  (3 shorter events, 0.0 us)
Async XLA Ops:
  6.5 137.5 %copy-start = (bf16[256,2048]{1,0:T(8,128)(2,1)S(1)}, bf16[256,2048]{1,0:T(8,128)(2,1)}, u32[]{:S(2)}) copy-start(bf16[256,2048]{1,0:T(8,128)(2,1)} %param.23) | copy-start | bytes 3145732
  6.5 177.3 %reduce-scatter.3.cloned.1.call-start = ((), (), s32[]{:S(2)}) async-start(), calls=%async_computation.2 | async-start | bytes 1179648 | tf_op jit(solution)/shard_map/reduce_scatter | solution.py:540
  17.5 127.0 %copy-start.3 = (bf16[256,2048]{1,0:T(8,128)(2,1)S(1)}, bf16[256,2048]{1,0:T(8,128)(2,1)}, u32[]{:S(2)}) copy-start(bf16[256,2048]{1,0:T(8,128)(2,1)} %param.24) | copy-start | bytes 3145732
  144.0 39.9 %copy-start.1 = (bf16[96,2048]{1,0:T(8,128)(2,1)S(1)}, bf16[96,2048]{1,0:T(8,128)(2,1)}, u32[]{:S(2)}) copy-start(bf16[96,2048]{1,0:T(8,128)(2,1)} %param.14) | copy-start | bytes 1179652
  144.4 40.7 %copy-start.4 = (f32[2048]{0:T(1024)S(1)}, f32[2048]{0:T(1024)}, u32[]{:S(2)}) copy-start(f32[2048]{0:T(1024)} %param.25) | copy-start | bytes 24580
  145.8 122.5 %reduce-scatter.5.cloned.1.call-start = ((), (), s32[]{:S(2)}) async-start(), calls=%async_computation.3 | async-start | bytes 9437184 | tf_op jit(solution)/shard_map/reduce_scatter | solution.py:559
  187.0 50.5 %copy-start.5 = (bf16[2048,512]{1,0:T(8,128)(2,1)S(1)}, bf16[2048,512]{1,0:T(8,128)(2,1)}, u32[]{:S(2)}) copy-start(bf16[2048,512]{1,0:T(8,128)(2,1)} %get-tuple-element.9) | copy-start | bytes 6291460
  317.3 2.6 copy-start.2
Sparse Core Ops, SparseCore 0:
  145.9 37.8 reduce-scatter.2
  248.7 19.6 reduce-scatter.4
